TPU v7x, 512 devices: a whole 4x4x16 slice. The times are simulated.
512 devices in a mesh: sp: 64 (over z, y), tp: 8 (over x, core).
Axes of the slice: x: 4, y: 4, z: 16, core: 2. Of those that a mesh axis runs over, the one named last changes fastest.
Arguments:
- tokens: bfloat16 [16384, 2048], P('sp'), may hold values from -6 to 6
- ln_gain: float32 [2048], replicated, may hold values from 0.1 to 1.9
- w_query_attn: bfloat16 [2048, 1024], P('sp', 'tp'), may hold values from -0.125 to 0.125
- w_key_attn: bfloat16 [2048, 1024], P('sp', 'tp'), may hold values from -0.125 to 0.125
- w_value_attn: bfloat16 [2048, 1024], P('sp', 'tp'), may hold values from -0.125 to 0.125
- w_query_delta: bfloat16 [2048, 1024], P('sp', 'tp'), may hold values from -0.125 to 0.125
- w_key_delta: bfloat16 [2048, 1024], P('sp', 'tp'), may hold values from -0.125 to 0.125
- w_value_delta: bfloat16 [2048, 1024], P('sp', 'tp'), may hold values from -0.125 to 0.125
- w_beta: bfloat16 [2048, 8], replicated, may hold values from -0.125 to 0.125
- w_decay: bfloat16 [2048, 8], replicated, may hold values from -0.125 to 0.125
- attn_bias: float32 [16], replicated, may hold values from -13 to 1
- decay_log: float32 [8], replicated, may hold values from -15 to -2
- beta_bias: float32 [8], replicated, may hold values from -7 to 1
- log_decay_extra: float32 [16384, 8], P('sp', 'tp'), may hold values from -0.7 to 0, as said below
- attn_gain: float32 [64], replicated, may hold values from 0.1 to 1.9
- delta_gain: float32 [128], replicated, may hold values from 0.1 to 1.9
- w_out_attn: bfloat16 [1024, 2048], P('tp', 'sp'), may hold values from -0.125 to 0.125
- w_out_delta: bfloat16 [1024, 2048], P('tp', 'sp'), may hold values from -0.125 to 0.125
Outputs:
- mixed_out: bfloat16 [16384, 2048], P(('sp', 'tp'))
Inputs may be any that keep to these rules, and one draw needn't show every extreme that they name: `log_decay_extra`: never positive.
All inputs are finite; a program needn't handle non-finite values.
Results may differ from a plain program's by a relative error of at most 0.015.
Values may be sent and summed in bfloat16 or wider, within the bound.
A program may use at most 128 MiB of HBM per device.

v0:
```python
import math
import jax
import jax.numpy as jnp
from jax import lax
from jax.sharding import Mesh
from jax.sharding import PartitionSpec as P

SB_DIM = 64
GDN_DIM = 128
DBLOCK = 64
SP = ("sp_0", "sp_1")
SP_TP = ("sp_0", "sp_1", "tp")


def side_by_side(arrays, axis, dim, along):
    widths = [a.shape[along] for a in arrays]
    both = jnp.concatenate(arrays, axis=along)
    result = lax.all_gather(both, axis, axis=dim, tiled=True)
    return tuple(jnp.split(result, [sum(widths[:k]) for k in range(1, len(widths))], axis=along))


def neutral_like(value, identity):
    return jax.tree.map(
        lambda a, e: jnp.broadcast_to(jnp.asarray(e, a.dtype), a.shape), value, identity
    )


def carried_in(value, axes, combine, identity):
    before = start = neutral_like(value, identity)
    running = value
    for axis in reversed(axes):
        length, index = (lax.axis_size(axis), lax.axis_index(axis))
        pieces = jax.tree.map(lambda part: lax.all_gather(part, axis), running)
        inside, running = (start, start)
        for k in range(length):
            passed = k < index
            running = combine(running, jax.tree.map(lambda part: part[k], pieces))
            inside = jax.tree.map(lambda new, old: jnp.where(passed, new, old), running, inside)
        before = combine(inside, before)
    return before


def turned_gather(arrays, axis, dims):
    turned = [jnp.moveaxis(a, dim, 0) for a, dim in zip(arrays, dims)]
    widths = [t[0].size for t in turned]
    both = jnp.concatenate([t.reshape(-1, w) for t, w in zip(turned, widths)], axis=1)
    result = lax.all_gather(both, axis, axis=0, tiled=True)
    pieces = jnp.split(result, [sum(widths[:k]) for k in range(1, len(widths))], axis=1)
    return tuple(
        (
            jnp.moveaxis(b.reshape(-1, *t.shape[1:]), 0, dim)
            for b, t, dim in zip(pieces, turned, dims)
        )
    )


def cut_along(value, dim, length):
    before, after = (value.shape[:dim], value.shape[dim + 1 :])
    return jnp.moveaxis(value.reshape(*before, length, -1, *after), dim, 0)


def summed_on_arrival(value, axis, dim):
    length = lax.axis_size(axis)
    pieces = lax.all_to_all(cut_along(value, dim, length), axis, 0, 0, tiled=True)
    return jnp.sum(pieces.astype(jnp.float32), axis=0)


def layer_normed(tok_rows, ln_gain):
    values = tok_rows.astype(jnp.float32)
    center = jnp.mean(values, axis=-1, keepdims=True)
    spread = jnp.mean(jnp.square(values - center), axis=-1, keepdims=True)
    return ((values - center) * lax.rsqrt(spread + 1e-05) * ln_gain).astype(jnp.bfloat16)


def rms_scaled(values, gain):
    return values * lax.rsqrt(jnp.mean(jnp.square(values), axis=-1, keepdims=True) + 1e-06) * gain


def unit_rows(values):
    return values * lax.rsqrt(jnp.sum(jnp.square(values), axis=-1, keepdims=True) + 1e-06)


def stick_block(carry, queries, query_pos, head_bias, key_block, value_block, key_first):
    outputs, log_kept = carry
    key_count = key_block.shape[0]
    heads = queries.shape[1]
    head_width = queries.shape[2]
    scores = jnp.einsum(
        "rhd,khd->hrk",
        queries,
        key_block.reshape(key_count, heads, head_width),
        preferred_element_type=jnp.float32,
    )
    scores = scores * head_width ** (-0.5) + head_bias[:, None, None]
    key_pos = key_first + jnp.arange(key_count, dtype=jnp.int32)
    visible = (key_pos[None, :] < query_pos[:, None]) & (key_pos[None, :] >= 0)
    lost = jnp.where(visible[None], -jax.nn.softplus(scores), 0.0)
    between = lax.cumsum(lost, axis=2, reverse=True) - lost + log_kept[:, :, None]
    weights = jnp.where(visible[None], jnp.exp(jax.nn.log_sigmoid(scores) + between), 0.0).astype(
        jnp.bfloat16
    )
    outputs = outputs + jnp.einsum(
        "hrk,khd->hrd",
        weights,
        value_block.reshape(key_count, heads, head_width),
        preferred_element_type=jnp.float32,
    )
    return (outputs, log_kept + jnp.sum(lost, axis=2))


def stick_span(carry, queries, query_pos, head_bias, keys, values, key_first):
    own_rows = queries.shape[0]
    length = keys.shape[0]
    widest = max(1, 1024 // own_rows)
    widest = 1 << widest.bit_length() - 1
    block = own_rows * math.gcd(widest, length // own_rows)
    blocks = length // block

    def one_turn(step_index, inner):
        block_index = blocks - 1 - step_index
        key_block = lax.dynamic_slice_in_dim(keys, block_index * block, block, 0)
        value_block = lax.dynamic_slice_in_dim(values, block_index * block, block, 0)
        return stick_block(
            inner,
            queries,
            query_pos,
            head_bias,
            key_block,
            value_block,
            key_first + block_index * block,
        )

    return lax.fori_loop(0, blocks, one_turn, carry)


def delta_parts(queries, keys, values, beta, decay):
    width = queries.shape[-2]
    key_width = queries.shape[-1]
    decay_sum = jnp.cumsum(decay, axis=-1)
    lower = jnp.tril(jnp.ones((width, width), dtype=bool))
    strict = jnp.tril(jnp.ones((width, width), dtype=bool), -1)
    differ = decay_sum[..., :, None] - decay_sum[..., None, :]
    decay_mask = jnp.where(lower, jnp.exp(jnp.where(lower, differ, 0.0)), 0.0)
    keys_beta = keys * beta[..., None]
    values_beta = values * beta[..., None]
    strict_mat = jnp.where(
        strict, jnp.einsum("...id,...jd->...ij", keys_beta, keys) * decay_mask, 0.0
    )
    right_side = jnp.concatenate([keys_beta * jnp.exp(decay_sum)[..., None], values_beta], axis=-1)
    solved = jax.scipy.linalg.solve_triangular(
        jnp.eye(width, dtype=jnp.float32) + strict_mat, right_side, lower=True
    )
    solve_keys = solved[..., :key_width]
    solve_values = solved[..., key_width:]
    query_key = jnp.einsum("...id,...jd->...ij", queries, keys) * decay_mask
    query_decayed = queries * jnp.exp(decay_sum)[..., None]
    keys_to_end = keys * jnp.exp(decay_sum[..., -1:] - decay_sum)[..., None]
    block_decay = jnp.exp(decay_sum[..., -1])
    return (solve_keys, solve_values, query_decayed, query_key, keys_to_end, block_decay)


def delta_update(state, block_parts):
    solve_keys, solve_values, query_decayed, query_key, keys_to_end, block_decay = block_parts
    fresh = solve_values - jnp.einsum("hcd,hde->hce", solve_keys, state)
    outputs = jnp.einsum("hcd,hde->hce", query_decayed, state)
    outputs = outputs + jnp.einsum("hij,hje->hie", query_key, fresh)
    state = state * block_decay[:, None, None] + jnp.einsum("hcd,hce->hde", keys_to_end, fresh)
    return (state, outputs)


def chain_combine(earlier, later):
    earlier_map, earlier_state = earlier
    later_map, later_state = later
    joined_map = jnp.einsum("hij,hjk->hik", later_map, earlier_map)
    joined_state = jnp.einsum("hij,hjk->hik", later_map, earlier_state) + later_state
    return (joined_map, joined_state)


def local(
    tokens,
    ln_gain,
    w_query_attn,
    w_key_attn,
    w_value_attn,
    w_query_delta,
    w_key_delta,
    w_value_delta,
    w_beta,
    w_decay,
    attn_bias,
    decay_log,
    beta_bias,
    log_decay_extra,
    attn_gain,
    delta_gain,
    w_out_attn,
    w_out_delta,
):
    row_count = tokens.shape[0]
    normed = layer_normed(tokens, ln_gain)
    segments = side_by_side(
        (w_query_attn, w_key_attn, w_value_attn, w_query_delta, w_key_delta, w_value_delta),
        SP,
        0,
        1,
    )
    summed = tuple(
        (jnp.dot(normed, segment, preferred_element_type=jnp.float32) for segment in segments)
    )
    attn_query, attn_key, attn_value, delta_query, delta_key, delta_value = [
        result.astype(jnp.bfloat16) for result in summed
    ]
    tp_pos = lax.axis_index("tp")
    sp_pos = lax.axis_index(SP)
    attn_heads = attn_query.shape[1] // SB_DIM
    delta_heads = delta_query.shape[1] // GDN_DIM
    positions = sp_pos * row_count + jnp.arange(row_count, dtype=jnp.int32)
    queries = attn_query.reshape(row_count, attn_heads, SB_DIM)
    head_bias = lax.dynamic_slice_in_dim(attn_bias, tp_pos * attn_heads, attn_heads, 0)
    carry = (
        jnp.zeros((attn_heads, row_count, SB_DIM), jnp.float32),
        jnp.zeros((attn_heads, row_count), jnp.float32),
    )
    every_key, every_value = side_by_side((attn_key, attn_value), SP, 0, 1)
    carry = stick_span(carry, queries, positions, head_bias, every_key, every_value, 0)
    attn_mixed = rms_scaled(carry[0], attn_gain).astype(jnp.bfloat16)
    head_first = tp_pos * delta_heads
    beta_cols = lax.dynamic_slice_in_dim(w_beta, head_first, delta_heads, 1)
    decay_cols = lax.dynamic_slice_in_dim(w_decay, head_first, delta_heads, 1)
    beta_pre = jnp.dot(normed, beta_cols, preferred_element_type=jnp.float32).astype(jnp.bfloat16)
    decay_pre = jnp.dot(normed, decay_cols, preferred_element_type=jnp.float32).astype(jnp.bfloat16)
    queries = unit_rows(
        jax.nn.silu(delta_query.astype(jnp.float32)).reshape(row_count, delta_heads, GDN_DIM)
    ) * GDN_DIM ** (-0.5)
    keys = unit_rows(
        jax.nn.silu(delta_key.astype(jnp.float32)).reshape(row_count, delta_heads, GDN_DIM)
    )
    values = jax.nn.silu(delta_value.astype(jnp.float32)).reshape(row_count, delta_heads, GDN_DIM)
    beta = jax.nn.sigmoid(
        beta_pre.astype(jnp.float32)
        + lax.dynamic_slice_in_dim(beta_bias, head_first, delta_heads, 0)
    )
    rates = jnp.exp(lax.dynamic_slice_in_dim(decay_log, head_first, delta_heads, 0))
    decay = -rates * jax.nn.softplus(decay_pre.astype(jnp.float32)) + log_decay_extra
    blocks = row_count // DBLOCK

    def to_blocks(array):
        return jnp.moveaxis(array.reshape((blocks, DBLOCK) + array.shape[1:]), 2, 0)

    parts = delta_parts(
        to_blocks(queries), to_blocks(keys), to_blocks(values), to_blocks(beta), to_blocks(decay)
    )
    sequence = tuple((jnp.moveaxis(piece_part, 1, 0) for piece_part in parts))
    eye_mat = jnp.eye(GDN_DIM, dtype=jnp.float32)

    def carry_map(accum, block_parts):
        transition, written = accum
        solve_keys, solve_values, query_decayed, query_key, keys_to_end, block_decay = block_parts
        step_matrix = block_decay[:, None, None] * eye_mat - jnp.einsum(
            "hcd,hce->hde", keys_to_end, solve_keys
        )
        transition = jnp.einsum("hij,hjk->hik", step_matrix, transition)
        written = jnp.einsum("hij,hjk->hik", step_matrix, written)
        written = written + jnp.einsum("hcd,hce->hde", keys_to_end, solve_values)
        return ((transition, written), None)

    neutral = (
        jnp.broadcast_to(eye_mat, (delta_heads, GDN_DIM, GDN_DIM)),
        jnp.zeros((delta_heads, GDN_DIM, GDN_DIM), jnp.float32),
    )
    own_chain, _ = lax.scan(carry_map, neutral, sequence)
    _, incoming = carried_in(own_chain, SP, chain_combine, neutral)
    _, outputs = lax.scan(delta_update, incoming, sequence)
    delta_raw = jnp.moveaxis(outputs, 0, 1).reshape(delta_heads, row_count, GDN_DIM)
    delta_mixed = rms_scaled(delta_raw, delta_gain).astype(jnp.bfloat16)
    full_attn, full_delta = turned_gather((w_out_attn, w_out_delta), SP, (1, 1))
    attn_weight3 = full_attn.reshape(attn_heads, SB_DIM, full_attn.shape[1])
    delta_weight3 = full_delta.reshape(delta_heads, GDN_DIM, full_delta.shape[1])
    result = jnp.einsum("hrd,hdn->rn", attn_mixed, attn_weight3, preferred_element_type=jnp.float32)
    mixed_rows = summed_on_arrival(
        (
            result
            + jnp.einsum(
                "hrd,hdn->rn", delta_mixed, delta_weight3, preferred_element_type=jnp.float32
            )
        ).astype(jnp.bfloat16),
        "tp",
        0,
    )
    return mixed_rows.astype(jnp.bfloat16)


def solution(mesh):
    split = Mesh(mesh.devices.reshape(16, 4, mesh.shape["tp"]), ("sp_0", "sp_1", "tp"))
    return jax.shard_map(
        local,
        mesh=split,
        in_specs=(
            P(SP, None),
            P(),
            P(SP, "tp"),
            P(SP, "tp"),
            P(SP, "tp"),
            P(SP, "tp"),
            P(SP, "tp"),
            P(SP, "tp"),
            P(),
            P(),
            P(),
            P(),
            P(),
            P(SP, "tp"),
            P(),
            P(),
            P("tp", SP),
            P("tp", SP),
        ),
        out_specs=P(SP_TP, None),
        check_vma=False,
    )
```

profile of v0, /device:TPU:1, one launch (start us, length us, event | category | flops | bytes accessed | tf_op | source)
XLA Modules:
  0.0 829.6 jit_solution(2809152960668360981)
XLA Ops:
  21.7 129.8 %all-gather.9.cloned.1.call-done = bf16[2048,768]{1,0:T(8,128)(2,1)} async-done(((bf16[32,768]{1,0:T(8,128)(2,1)}), bf16[2048,768]{1,0:T(8,128)(2,1)}) %all-gather.9.cloned.1.call-update) | async-done | bytes 3145744 | tf_op jit(solution)/shard_map/all_gather | solution.py:18
  153.3 19.7 %custom-call.4 = f32[4,1,64,64]{2,3,1,0:T(8,128)S(1)} custom-call(f32[4,1,64,64]{3,2,1,0:T(8,128)S(1)} %fusion.60), custom_call_target="InvertDiagBlocksLowerTriangular" | custom-call | tf_op jit(solution)/shard_map/jit(_solve_triangular)/vmap()/triangular_solve | solution.py:150
  175.2 7.6 while.42
  182.9 9.2 %all-gather = bf16[4,128,128]{2,1,0:T(8,128)(2,1)S(1)} all-gather(bf16[1,128,128]{2,1,0:T(8,128)(2,1)S(1)} %get-tuple-element.235), channel_id=2, replica_groups=mesh['sp_0'=16,'sp_1'=4,'tp'=8] {'sp_1'}, dimensions={0}, use_global_device_ids=true | all-gather | bytes 163840 | tf_op jit(solution)/shard_map/all_gather | solution.py:33
  192.0 9.8 %all-gather.2 = f32[4,128,128]{2,1,0:T(8,128)S(1)} all-gather(f32[1,128,128]{2,1,0:T(8,128)S(1)} %get-tuple-element.236), channel_id=4, replica_groups=mesh['sp_0'=16,'sp_1'=4,'tp'=8] {'sp_1'}, dimensions={0}, use_global_device_ids=true | all-gather | bytes 327680 | tf_op jit(solution)/shard_map/all_gather | solution.py:33
  207.0 81.6 %all-gather.13.cloned.1.call-done = bf16[2048,256]{1,0:T(8,128)(2,1)} async-done(((bf16[32,256]{1,0:T(8,128)(2,1)}), bf16[2048,256]{1,0:T(8,128)(2,1)}) %all-gather.13.cloned.1.call-update) | async-done | bytes 1048592 | tf_op jit(solution)/shard_map/all_gather | solution.py:47
  292.4 23.6 %all-gather.1 = bf16[2048,128]{1,0:T(8,128)(2,1)S(1)} all-gather(bf16[128,128]{1,0:T(8,128)(2,1)S(1)} %fusion.140), channel_id=3, replica_groups=mesh['sp_0'=16,'sp_1'=4,'tp'=8] {'sp_0'}, dimensions={0}, use_global_device_ids=true | all-gather | bytes 557056 | tf_op jit(solution)/shard_map/all_gather | solution.py:33
  317.6 39.7 %all-gather.15.cloned.1.call-done = f32[2048,128]{1,0:T(8,128)} async-done(((f32[128,128]{1,0:T(8,128)}), f32[2048,128]{1,0:T(8,128)}) %all-gather.15.cloned.1.call-update) | async-done | bytes 1048592 | tf_op jit(solution)/shard_map/all_gather | solution.py:33
  373.3 6.9 while.41
  380.5 145.7 %all-gather.11.cloned.1.call-done = bf16[16384,256]{0,1:T(8,128)(2,1)} async-done(((bf16[256,256]{0,1:T(8,128)(2,1)}), bf16[16384,256]{0,1:T(8,128)(2,1)}) %all-gather.11.cloned.1.call-update) | async-done | bytes 8388624 | tf_op jit(solution)/shard_map/all_gather | solution.py:18
  526.2 5.8 fusion.199
  532.0 259.6 %while.43 = (s32[]{:T(128)}, f32[2,256,64]{1,2,0:T(8,128)S(1)}, f32[2,256]{1,0:T(2,128)S(1)}, bf16[16384,128]{0,1:T(8,128)(2,1)}, bf16[256,2,64]{0,2,1:T(8,128)(...) while((s32[]{:T(128)}, f32[2,256,64]{1,2,0:T(8,128)S(1)}, ...), condition=%wide.region_6.7_spmd.clone, body=%wide.region_2.6_spmd.clone.sunk | while | flops 215584000 | bytes 44771616 | solution.py:133
  536.5 5.0 fusion.312
  552.7 5.0 fusion.312
  569.0 5.0 fusion.312
  585.2 5.0 fusion.312
  592.4 4.2 fusion.314
  601.4 5.0 fusion.312
  617.7 5.0 fusion.312
  633.9 5.0 fusion.312
  650.1 5.0 fusion.312
  657.3 4.2 fusion.314
  666.3 5.0 fusion.312
  673.5 4.2 fusion.314
  682.6 5.0 fusion.312
  698.8 5.0 fusion.312
  715.0 5.0 fusion.312
  731.2 5.0 fusion.312
  747.5 5.0 fusion.312
  763.7 5.0 fusion.312
  779.9 5.0 fusion.312
  793.3 28.9 %all_to_all.5 = bf16[8,32,2048]{2,1,0:T(8,128)(2,1)S(1)} all-to-all(bf16[8,32,2048]{2,1,0:T(8,128)(2,1)S(1)} %bitcast.318), channel_id=1, replica_groups=mesh['sp_0'=16,'sp_1'=4,'tp'=8] {'tp'}, dimensions={0} | all-to-all | bytes 2097152 | tf_op jit(solution)/shard_map/all_to_all | solution.py:64
  (449 shorter events, 226.4 us)
Async XLA Ops:
  6.5 11.4 %copy-start = (bf16[2048,8]{0,1:T(8,128)(2,1)S(1)}, bf16[2048,8]{0,1:T(8,128)(2,1)}, u32[]{:S(2)}) copy-start(bf16[2048,8]{0,1:T(8,128)(2,1)} %param.33) | copy-start | bytes 98308
  6.5 11.0 %copy-start.3 = (bf16[256,2048]{1,0:T(8,128)(2,1)S(1)}, bf16[256,2048]{1,0:T(8,128)(2,1)}, u32[]{:S(2)}) copy-start(bf16[256,2048]{1,0:T(8,128)(2,1)} %param.24) | copy-start | bytes 3145732
  6.5 9.6 %copy-start.11 = (f32[8]{0:T(128)S(1)}, f32[8]{0:T(128)}, u32[]{:S(2)}) copy-start(f32[8]{0:T(128)} %param.35) | copy-start | bytes 100
  6.5 11.0 %copy-start.7 = (f32[2048]{0:T(1024)S(1)}, f32[2048]{0:T(1024)}, u32[]{:S(2)}) copy-start(f32[2048]{0:T(1024)} %param.25) | copy-start | bytes 24580
  6.5 144.9 %all-gather.9.cloned.1.call-start = ((), (), s32[]{:S(2)}) async-start(), calls=%async_computation.1 | async-start | bytes 3194880 | tf_op jit(solution)/shard_map/all_gather | solution.py:18
  11.5 277.0 %all-gather.13.cloned.1.call-start = ((), (), s32[]{:S(2)}) async-start(), calls=%async_computation.3 | async-start | bytes 1064960 | tf_op jit(solution)/shard_map/all_gather | solution.py:47
  12.9 344.4 %all-gather.15.cloned.1.call-start = ((), (), s32[]{:S(2)}) async-start(), calls=%async_computation.4 | async-start | bytes 1114112 | tf_op jit(solution)/shard_map/all_gather | solution.py:33
  14.5 3.9 copy-start.8
  17.6 2.6 copy-start.12
  202.0 4.9 copy-start.13
  203.0 323.2 %all-gather.11.cloned.1.call-start = ((), (), s32[]{:S(2)}) async-start(), calls=%async_computation.2 | async-start | bytes 8519680 | tf_op jit(solution)/shard_map/all_gather | solution.py:18
  317.6 55.6 %copy-start.5 = (f32[128,128]{1,0:T(8,128)S(1)}, f32[128,128]{1,0:T(8,128)}, u32[]{:S(2)}) copy-start(f32[128,128]{1,0:T(8,128)} %convolution_add_fusion.20) | copy-start | bytes 196612
  372.0 8.4 %copy-start.9 = (f32[128]{0:T(128)S(1)}, f32[128]{0:T(128)}, u32[]{:S(2)}) copy-start(f32[128]{0:T(128)} %param.39) | copy-start | bytes 1540
  532.0 259.7 %copy-start.10 = (f32[64]{0:T(128)S(1)}, f32[64]{0:T(128)}, u32[]{:S(2)}) copy-start(f32[64]{0:T(128)} %param.38) | copy-start | bytes 772
  536.5 5.0 copy-start.1
  541.8 1.9 copy-start.2
  552.7 5.0 copy-start.1
  558.0 1.9 copy-start.2
  569.0 5.0 copy-start.1
  585.2 5.0 copy-start.1
  601.4 5.0 copy-start.1
  617.7 5.0 copy-start.1
  633.9 5.0 copy-start.1
  650.1 5.0 copy-start.1
  666.3 5.0 copy-start.1
  682.6 5.0 copy-start.1
  698.8 5.0 copy-start.1
  715.0 5.0 copy-start.1
  731.2 5.0 copy-start.1
  747.5 5.0 copy-start.1
  763.7 5.0 copy-start.1
  779.9 5.0 copy-start.1
  (16 other events, 29.0 us)
Sparse Core Ops, SparseCore 0:
  11.7 139.7 all-gather.8
  154.3 134.1 all-gather.12
  290.6 66.6 all-gather.14
  360.1 166.0 all-gather.10
where the time goes:
time: 832 us; the launch traced here: 830 us
  waiting for transfers between devices  397 us (48%)
  other arithmetic  184 us (22%)
  matrix products  93.2 us (11%)
  blocking collectives  71.5 us (9%)
  local copies, waits for them, and re-layouts  67.3 us (8%)
  between operations  14.3 us (2%)
    all_gather x2, waiting for transfers between devices, side_by_side(): result = lax.all_gather(both, axis, axis=dim, tiled=True)  275 us
    all_gather x1, waiting for transfers between devices, turned_gather(): result = lax.all_gather(both, axis, axis=0, tiled=True)  81.6 us
    another operation x32, other arithmetic  81.2 us
    convert_element_type x16, other arithmetic, stick_block(): jnp.where(visible[None], jnp.exp(jax.nn.log_sigmoid(scores) + between), 0.0)  67.1 us
    dot_general x16, matrix products, stick_block(): jnp.einsum('rhd,khd->hrk', queries, key_block.reshape(key_count, heads, h...  48.4 us
    all_gather x3, blocking collectives, carried_in(): pieces = jax.tree.map(lambda part: lax.all_gather(part, axis), running)  42.6 us
    all_gather x1, waiting for transfers between devices, carried_in(): pieces = jax.tree.map(lambda part: lax.all_gather(part, axis), running)  39.7 us
    another operation x16, local copies, waits for them, and re-layouts, stick_block(): lax.cumsum(lost, axis=2, reverse=True) - lost + log_kept[:, :, None]  30.7 us
  transfers between devices with their start and end apart: 4, of which 4 were waited for; matrix products, arithmetic and copies ran while one was open for 9% of the time, Pallas kernels for 0%

commit v1 on v0

--- a/solution.py
+++ b/solution.py
@@ -44,7 +44,8 @@
     turned = [jnp.moveaxis(a, dim, 0) for a, dim in zip(arrays, dims)]
     widths = [t[0].size for t in turned]
     both = jnp.concatenate([t.reshape(-1, w) for t, w in zip(turned, widths)], axis=1)
-    result = lax.all_gather(both, axis, axis=0, tiled=True)
+    sent = jnp.stack([both] * lax.axis_size(axis))
+    result = jnp.concatenate(lax.all_to_all(sent, axis, 0, 0), axis=0)
     pieces = jnp.split(result, [sum(widths[:k]) for k in range(1, len(widths))], axis=1)
     return tuple(
         (

time: 832 us -> 773 us (0.929)
  waiting for transfers between devices: 397 us -> 304 us
  matrix products: 93.2 us -> 110 us
    all_gather x1 -> x0, waiting for transfers between devices: 81.6 us -> none  [turned_gather(): result = lax.all_gather(both, axis, axis=0, tiled=True)]
    all_to_all x0 -> x1, waiting for transfers between devices: none -> 41 us  [turned_gather(): result = jnp.concatenate(lax.all_to_all(sent, axis, 0, 0), axis=0)]
    all_gather x1, waiting for transfers between devices: 39.7 us -> 0.02 us  [carried_in(): pieces = jax.tree.map(lambda part: lax.all_gather(part, axis), running)]
    dot_general x16, matrix products: 48.4 us -> 61.5 us  [stick_block(): jnp.einsum('rhd,khd->hrk', queries, key_block.reshape(key_count, heads, h...]
    all_gather x2, waiting for transfers between devices: 275 us -> 263 us  [side_by_side(): result = lax.all_gather(both, axis, axis=dim, tiled=True)]
    all_to_all x0 -> x1, starting transfers between devices: none -> 8.38 us  [turned_gather(): result = jnp.concatenate(lax.all_to_all(sent, axis, 0, 0), axis=0)]
  transfers between devices with their start and end apart: 4 -> 4, of which waited for: 4 -> 3; matrix products, arithmetic and copies ran while one was open for 9% -> 6% of each run, Pallas kernels for 0% -> 0%
where the time goes in v1:
time: 773 us; the launch traced here: 769 us
  waiting for transfers between devices  304 us (39%)
  other arithmetic  184 us (24%)
  matrix products  110 us (14%)
  blocking collectives  76.6 us (10%)
  local copies, waits for them, and re-layouts  69.4 us (9%)
  between operations  14.4 us (2%)
  starting transfers between devices  8.46 us (1%)
    all_gather x2, waiting for transfers between devices, side_by_side(): result = lax.all_gather(both, axis, axis=dim, tiled=True)  263 us
    another operation x32, other arithmetic  81.2 us
    convert_element_type x16, other arithmetic, stick_block(): jnp.where(visible[None], jnp.exp(jax.nn.log_sigmoid(scores) + between), 0.0)  67.1 us
    dot_general x16, matrix products, stick_block(): jnp.einsum('rhd,khd->hrk', queries, key_block.reshape(key_count, heads, h...  61.5 us
    all_gather x3, blocking collectives, carried_in(): pieces = jax.tree.map(lambda part: lax.all_gather(part, axis), running)  47.7 us
    all_to_all x1, waiting for transfers between devices, turned_gather(): result = jnp.concatenate(lax.all_to_all(sent, axis, 0, 0), axis=0)  41 us
    another operation x16, local copies, waits for them, and re-layouts, stick_block(): lax.cumsum(lost, axis=2, reverse=True) - lost + log_kept[:, :, None]  31 us
    all_to_all x1, blocking collectives, summed_on_arrival(): lax.all_to_all(cut_along(value, dim, length), axis, 0, 0, tiled=True)  28.9 us
  transfers between devices with their start and end apart: 4, of which 3 were waited for; matrix products, arithmetic and copies ran while one was open for 6% of the time, Pallas kernels for 0%

profile of v1, /device:TPU:1, one launch (start us, length us, event | category | flops | bytes accessed | tf_op | source)
XLA Modules:
  0.0 769.5 jit_solution(12442487450140274144)
XLA Ops:
  20.7 130.6 %all-gather.8.cloned.1.call-done = bf16[2048,768]{1,0:T(8,128)(2,1)} async-done(((bf16[32,768]{1,0:T(8,128)(2,1)}), bf16[2048,768]{1,0:T(8,128)(2,1)}) %all-gather.8.cloned.1.call-update) | async-done | bytes 3145744 | tf_op jit(solution)/shard_map/all_gather | solution.py:18
  153.3 19.7 %custom-call.4 = f32[4,1,64,64]{2,3,1,0:T(8,128)S(1)} custom-call(f32[4,1,64,64]{3,2,1,0:T(8,128)S(1)} %fusion.60), custom_call_target="InvertDiagBlocksLowerTriangular" | custom-call | tf_op jit(solution)/shard_map/jit(_solve_triangular)/vmap()/triangular_solve | solution.py:151
  175.8 7.6 while.42
  183.5 9.1 %all-gather = bf16[4,128,128]{2,1,0:T(8,128)(2,1)S(1)} all-gather(bf16[1,128,128]{2,1,0:T(8,128)(2,1)S(1)} %get-tuple-element.235), channel_id=2, replica_groups=mesh['sp_0'=16,'sp_1'=4,'tp'=8] {'sp_1'}, dimensions={0}, use_global_device_ids=true | all-gather | bytes 163840 | tf_op jit(solution)/shard_map/all_gather | solution.py:33
  192.6 9.4 %all-gather.2 = f32[4,128,128]{2,1,0:T(8,128)S(1)} all-gather(f32[1,128,128]{2,1,0:T(8,128)S(1)} %get-tuple-element.236), channel_id=4, replica_groups=mesh['sp_0'=16,'sp_1'=4,'tp'=8] {'sp_1'}, dimensions={0}, use_global_device_ids=true | all-gather | bytes 327680 | tf_op jit(solution)/shard_map/all_gather | solution.py:33
  208.3 8.4 %all-to-all-start = ((bf16[64,32,256]{2,1,0:T(8,128)(2,1)}), bf16[64,32,256]{2,1,0:T(8,128)(2,1)S(1)}, u32[]{:S(2)}, u32[]{:S(2)}) async-start(bf16[64,32,256]{2,1,0:T(8,128)(2,1)} %stack.2), calls=%async_computation | async-start | bytes 2097152 | tf_op jit(solution)/shard_map/all_to_all | solution.py:48
  217.4 41.0 %all-to-all-done = bf16[64,32,256]{2,1,0:T(8,128)(2,1)S(1)} async-done(((bf16[64,32,256]{2,1,0:T(8,128)(2,1)}), bf16[64,32,256]{2,1,0:T(8,128)(2,1)S(1)}, u32[]{:S(2)}, u32[]{:S(2)}) %all-to-all-start) | async-done | bytes 1048608 | tf_op jit(solution)/shard_map/all_to_all | solution.py:48
  261.4 29.3 %all-gather.1 = bf16[2048,128]{1,0:T(8,128)(2,1)S(1)} all-gather(bf16[128,128]{1,0:T(8,128)(2,1)S(1)} %fusion.140), channel_id=3, replica_groups=mesh['sp_0'=16,'sp_1'=4,'tp'=8] {'sp_0'}, dimensions={0}, use_global_device_ids=true | all-gather | bytes 557056 | tf_op jit(solution)/shard_map/all_gather | solution.py:33
  309.0 10.7 %while.41 = (s32[]{:T(128)}, f32[1,128,128]{2,1,0:T(8,128)S(1)}, f32[4,1,64,128]{3,2,1,0:T(8,128)S(1)}, f32[4,1]{0,1:T(1,128)S(1)}, bf16[4,1,64,128]{3,2,1,0:T(8...) while((s32[]{:T(128)}, f32[1,128,128]{2,1,0:T(8,128)S(1)}, ...), condition=%wide.region_14.15_spmd, body=%wide.region_13.14_spmd.sunk | while | flops 7397378 | bytes 510077 | solution.py:274
  320.0 132.8 %all-gather.10.cloned.1.call-done = bf16[16384,256]{0,1:T(8,128)(2,1)} async-done(((bf16[256,256]{0,1:T(8,128)(2,1)}), bf16[16384,256]{0,1:T(8,128)(2,1)}) %all-gather.10.cloned.1.call-update) | async-done | bytes 8388624 | tf_op jit(solution)/shard_map/all_gather | solution.py:18
  452.8 5.8 fusion.199
  458.6 273.0 %while.43 = (s32[]{:T(128)}, f32[2,256,64]{1,2,0:T(8,128)S(1)}, f32[2,256]{1,0:T(2,128)S(1)}, bf16[16384,128]{0,1:T(8,128)(2,1)}, bf16[256,2,64]{0,2,1:T(8,128)(...) while((s32[]{:T(128)}, f32[2,256,64]{1,2,0:T(8,128)S(1)}, ...), condition=%wide.region_6.7_spmd.clone, body=%wide.region_2.6_spmd.clone.sunk | while | flops 215584000 | bytes 44771616 | solution.py:134
  463.9 5.0 fusion.312
  471.1 4.2 fusion.314
  481.0 5.0 fusion.312
  488.2 4.2 fusion.314
  498.0 5.0 fusion.312
  505.3 4.2 fusion.314
  515.1 5.0 fusion.312
  532.2 5.0 fusion.312
  549.2 5.0 fusion.312
  566.3 5.0 fusion.312
  583.4 5.0 fusion.312
  600.4 5.0 fusion.312
  617.5 5.0 fusion.312
  634.5 5.0 fusion.312
  651.6 5.0 fusion.312
  668.7 5.0 fusion.312
  685.7 5.0 fusion.312
  702.8 5.0 fusion.312
  719.8 5.0 fusion.312
  733.3 28.9 %all_to_all.10 = bf16[8,32,2048]{2,1,0:T(8,128)(2,1)S(1)} all-to-all(bf16[8,32,2048]{2,1,0:T(8,128)(2,1)S(1)} %bitcast.319), channel_id=1, replica_groups=mesh['sp_0'=16,'sp_1'=4,'tp'=8] {'tp'}, dimensions={0} | all-to-all | bytes 2097152 | tf_op jit(solution)/shard_map/all_to_all | solution.py:65
  (479 shorter events, 245.1 us)
Async XLA Ops:
  6.5 10.5 %copy-start = (bf16[2048,8]{0,1:T(8,128)(2,1)S(1)}, bf16[2048,8]{0,1:T(8,128)(2,1)}, u32[]{:S(2)}) copy-start(bf16[2048,8]{0,1:T(8,128)(2,1)} %param.33) | copy-start | bytes 98308
  6.5 10.1 %copy-start.3 = (bf16[256,2048]{1,0:T(8,128)(2,1)S(1)}, bf16[256,2048]{1,0:T(8,128)(2,1)}, u32[]{:S(2)}) copy-start(bf16[256,2048]{1,0:T(8,128)(2,1)} %param.24) | copy-start | bytes 3145732
  6.5 10.1 %copy-start.19 = (f32[2048]{0:T(1024)S(1)}, f32[2048]{0:T(1024)}, u32[]{:S(2)}) copy-start(f32[2048]{0:T(1024)} %param.25) | copy-start | bytes 24580
  6.5 144.8 %all-gather.8.cloned.1.call-start = ((), (), s32[]{:S(2)}) async-start(), calls=%async_computation.2 | async-start | bytes 3194880 | tf_op jit(solution)/shard_map/all_gather | solution.py:18
  11.5 281.3 %all-gather.12.cloned.1.call-start = ((), (), s32[]{:S(2)}) async-start(), calls=%async_computation.4 | async-start | bytes 1114112 | tf_op jit(solution)/shard_map/all_gather | solution.py:33
  20.7 153.8 %copy-start.16 = (f32[4,64]{1,0:T(4,128)}, f32[4,64]{1,0:T(4,128)S(1)}, u32[]{:S(2)}) copy-start(f32[4,64]{1,0:T(4,128)S(1)} %get-tuple-element.395) | copy-start | bytes 3076
  183.5 9.1 %copy-start.10 = (bf16[4,1,64,128]{3,2,1,0:T(8,128)(2,1)}, bf16[4,1,64,128]{3,2,1,0:T(8,128)(2,1)S(1)}, u32[]{:S(2)}) copy-start(bf16[4,1,64,128]{3,2,1,0:T(8,128)(2,1)S(1)} %get-tuple-element.672) | copy-start | bytes 196612
  183.5 18.5 %copy-start.24 = (f32[4,1]{0,1:T(1,128)}, f32[4,1]{0,1:T(1,128)S(1)}, u32[]{:S(2)}) copy-start(f32[4,1]{0,1:T(1,128)S(1)} %get-tuple-element.675) | copy-start | bytes 52
  192.6 13.7 %copy-start.6 = (bf16[4,128,128]{2,1,0:T(8,128)(2,1)}, bf16[4,128,128]{2,1,0:T(8,128)(2,1)S(1)}, u32[]{:S(2)}) copy-start(bf16[4,128,128]{2,1,0:T(8,128)(2,1)S(1)} %all-gather) | copy-start | bytes 393220
  202.4 5.9 copy-start.13
  203.2 249.6 %all-gather.10.cloned.1.call-start = ((), (), s32[]{:S(2)}) async-start(), calls=%async_computation.3 | async-start | bytes 8519680 | tf_op jit(solution)/shard_map/all_gather | solution.py:18
  206.3 10.4 %copy-start.28 = (f32[16]{0:T(128)S(1)}, f32[16]{0:T(128)}, u32[]{:S(2)}) copy-start(f32[16]{0:T(128)} %param.34) | copy-start | bytes 196
  208.3 50.1 %all-to-all-start = ((bf16[64,32,256]{2,1,0:T(8,128)(2,1)}), bf16[64,32,256]{2,1,0:T(8,128)(2,1)S(1)}, u32[]{:S(2)}, u32[]{:S(2)}) async-start(bf16[64,32,256]{2,1,0:T(8,128)(2,1)} %stack.2), calls=%async_computation | async-start | bytes 2097152 | tf_op jit(solution)/shard_map/all_to_all | solution.py:48
  292.8 16.0 %copy-start.8 = (f32[128,128]{1,0:T(8,128)S(1)}, f32[128,128]{1,0:T(8,128)}, u32[]{:S(2)}) copy-start(f32[128,128]{1,0:T(8,128)} %convolution_add_fusion.20) | copy-start | bytes 196612
  292.8 16.0 %copy-start.12 = (bf16[128,128]{1,0:T(8,128)(2,1)S(1)}, bf16[128,128]{1,0:T(8,128)(2,1)}, u32[]{:S(2)}) copy-start(bf16[128,128]{1,0:T(8,128)(2,1)} %copy-done.11) | copy-start | bytes 98308
  292.8 16.0 %copy-start.14 = (bf16[128,128]{1,0:T(8,128)(2,1)S(1)}, bf16[128,128]{1,0:T(8,128)(2,1)}, u32[]{:S(2)}) copy-start(bf16[128,128]{1,0:T(8,128)(2,1)} %copy-done.13) | copy-start | bytes 98308
  292.8 16.1 %copy-start.9 = (f32[4,1,64,128]{3,2,1,0:T(8,128)S(1)}, f32[4,1,64,128]{3,2,1,0:T(8,128)}, u32[]{:S(2)}) copy-start(f32[4,1,64,128]{3,2,1,0:T(8,128)} %custom-call.8) | copy-start | bytes 393220
  292.8 16.1 %copy-start.25 = (f32[4,1]{0,1:T(1,128)S(1)}, f32[4,1]{0,1:T(1,128)}, u32[]{:S(2)}) copy-start(f32[4,1]{0,1:T(1,128)} %copy-done.24) | copy-start | bytes 52
  307.6 12.3 %copy-start.23 = (f32[128]{0:T(128)S(1)}, f32[128]{0:T(128)}, u32[]{:S(2)}) copy-start(f32[128]{0:T(128)} %param.39) | copy-start | bytes 1540
  320.0 138.6 %copy-start.18 = (f32[2]{0:T(128)S(1)}, f32[2]{0:T(128)}, u32[]{:S(2)}) copy-start(f32[2]{0:T(128)} %dynamic_slice.62) | copy-start | bytes 28
  458.6 273.1 %copy-start.26 = (f32[64]{0:T(128)S(1)}, f32[64]{0:T(128)}, u32[]{:S(2)}) copy-start(f32[64]{0:T(128)} %param.38) | copy-start | bytes 772
  463.9 5.0 copy-start.1
  481.0 5.0 copy-start.1
  498.0 5.0 copy-start.1
  515.1 5.0 copy-start.1
  532.2 5.0 copy-start.1
  549.2 5.0 copy-start.1
  583.3 5.0 copy-start.1
  600.4 5.0 copy-start.1
  634.5 5.0 copy-start.1
  651.6 5.0 copy-start.1
  685.7 5.0 copy-start.1
  (31 other events, 85.0 us)
Sparse Core Ops, SparseCore 0:
  11.6 139.7 all-gather.7
  203.3 85.7 all-gather.11
  292.0 160.6 all-gather.9
